TPU v7x, 256 devices: a whole 4x4x8 slice. The times are simulated.
256 devices in a mesh: sp: 16 (over y, x), tp: 16 (over z, core).
Axes of the slice: x: 4, y: 4, z: 8, core: 2. Of those that a mesh axis runs over, the one named last changes fastest.
Arguments:
- query_input: bfloat16 [1024, 4096], P('tp', 'sp'), may hold values from -6 to 6
- key_input: bfloat16 [1024, 4096], P('tp', 'sp'), may hold values from -6 to 6
- retrieved_content_matrix: bfloat16 [1024, 4096], P('tp', 'sp'), may hold values from -6 to 6
- gate_input: bfloat16 [1024, 4096], P('tp', 'sp'), may hold values from -6 to 6
- log_decay: float32 [2, 16, 4096], P(None, 'tp', 'sp'), may hold values from -2 to 0
- residual: bfloat16 [4096, 2048], P(('sp', 'tp')), may hold values from -6 to 6
- out_weight: bfloat16 [1024, 2048], replicated, may hold values from -0.1875 to 0.1875
- norm_gain: bfloat16 [2048], replicated, may hold values from 0.099609375 to 1.8984375
- routes: int32 [4096, 2], P(('sp', 'tp')), may hold values from 0 to 15, all different within a row; in each aligned block of 16 rows (0 to 15, 16 to 31, ...) at most 3 rows name the same one
- route_weight: float32 [4096, 2], P(('sp', 'tp')), may hold values from 0.1 to 1
- gate_weight: bfloat16 [16, 2048, 5504], P('sp', None, 'tp'), may hold values from -0.125 to 0.125
- up_weight: bfloat16 [16, 2048, 5504], P('sp', None, 'tp'), may hold values from -0.125 to 0.125
- down_weight: bfloat16 [16, 5504, 2048], P('sp', 'tp'), may hold values from -0.078125 to 0.078125
Outputs:
- output: bfloat16 [4096, 2048], P(('sp', 'tp'))
Inputs may be any that keep to these rules, and one draw needn't show every extreme that they name: `routes`: each row names 2 different experts. In each aligned block of 16 rows no expert is named by more than 3 rows, a bound that some block reaches.
All inputs are finite; a program needn't handle non-finite values.
Results may differ from a plain program's by a relative error of at most 0.015.
Values may be sent and summed in bfloat16 or wider, within the bound.
A program may use at most 64 MiB of HBM per device.

v0:
```python
import jax
import jax.numpy as jnp
from jax import lax
from jax.sharding import Mesh
from jax.sharding import PartitionSpec as P

HEAD_DIM = 64
TP = ("tp_0", "tp_1")
SP_TP = ("sp", "tp_0", "tp_1")


def sent_together(arrays, axis, dim, along):
    columns = [a.reshape(*a.shape[:along], -1) for a in arrays]
    both = jnp.concatenate(columns, axis=along)
    whole, at, done = (lax.all_gather(both, axis, axis=dim, tiled=True), 0, [])
    for a, column in zip(arrays, columns):
        share = whole[..., at : at + column.shape[along]]
        done.append(share.reshape(*share.shape[:along], *a.shape[along:]))
        at += column.shape[along]
    return tuple(done)


def in_blocks(x, dim, size):
    before, after = (x.shape[:dim], x.shape[dim + 1 :])
    return jnp.moveaxis(x.reshape(*before, size, -1, *after), dim, 0)


def sum_by_chip(x, chips, core, dim):
    sizes = (lax.axis_size(chips), lax.axis_size(core))
    tiles = in_blocks(x, dim, sizes[0] * sizes[1])
    inside = tiles.shape[1:]
    tiles = tiles.reshape(*sizes, *inside).swapaxes(0, 1).reshape(-1, *inside)
    tiles = lax.psum_scatter(tiles, core, scatter_dimension=0, tiled=True)
    return lax.psum_scatter(tiles, chips, scatter_dimension=0, tiled=True)[0]


def head_norm(values, mesh_axis):
    centred = values - jnp.mean(values, axis=mesh_axis, keepdims=True)
    return centred * lax.rsqrt(jnp.mean(centred * centred, axis=mesh_axis, keepdims=True) + 1e-06)


def on_device(
    query_input,
    key_input,
    retrieved_content_matrix,
    gate_input,
    log_decay,
    residual,
    out_weight,
    norm_gain,
    routes,
    route_weight,
    gate_weight,
    up_weight,
    down_weight,
):
    heads_here = query_input.shape[0] // HEAD_DIM
    length = query_input.shape[1]
    queries = query_input.reshape(heads_here, HEAD_DIM, length)
    all_keys = key_input.reshape(heads_here, HEAD_DIM, length)
    all_values = retrieved_content_matrix.reshape(heads_here, HEAD_DIM, length)
    forward_log = log_decay[0]
    backward_log = log_decay[1]
    forward_prefix = jnp.cumsum(forward_log, axis=-1)
    backward_prefix = jnp.cumsum(backward_log, axis=-1) - backward_log
    forward_total = forward_prefix[:, -1]
    backward_total = jnp.sum(backward_log, axis=-1)
    wide_keys = all_keys.astype(jnp.float32)
    wide_values = all_values.astype(jnp.float32)
    forward_keys = wide_keys * jnp.exp(forward_total[:, None] - forward_prefix)[:, None, :]
    backward_keys = wide_keys * jnp.exp(backward_prefix)[:, None, :]
    local_forward = jnp.einsum("hds,hes->hde", forward_keys, wide_values)
    backward_local = jnp.einsum("hds,hes->hde", backward_keys, wide_values)
    fwd_totals, bwd_totals, fwd_states, bwd_states = tuple(
        (
            part.astype(jnp.float32)
            for part in sent_together(
                (
                    forward_total[None].astype(jnp.bfloat16),
                    backward_total[None].astype(jnp.bfloat16),
                    local_forward[None].astype(jnp.bfloat16),
                    backward_local[None].astype(jnp.bfloat16),
                ),
                "sp",
                0,
                2,
            )
        )
    )
    position = lax.axis_index("sp")
    bucket_locations = jnp.arange(fwd_totals.shape[0])
    forward_running = jnp.cumsum(fwd_totals, axis=0)
    before_mine = lax.dynamic_index_in_dim(forward_running - fwd_totals, position, 0, False)
    forward_decay_weight = jnp.where(
        (bucket_locations < position)[:, None],
        jnp.exp(jnp.minimum(before_mine[None, :] - forward_running, 0.0)),
        0.0,
    )
    forward_in = jnp.sum(forward_decay_weight[:, :, None, None] * fwd_states, axis=0)
    backward_running = jnp.cumsum(bwd_totals, axis=0)
    through_mine = lax.dynamic_index_in_dim(backward_running, position, 0, False)
    backward_weight = jnp.where(
        (bucket_locations > position)[:, None],
        jnp.exp(jnp.minimum(backward_running - bwd_totals - through_mine[None, :], 0.0)),
        0.0,
    )
    backward_in = jnp.sum(backward_weight[:, :, None, None] * bwd_states, axis=0)
    block_size = min(512, length)
    block_count = length // block_size
    offsets = jnp.arange(length)

    def block_output(block):
        start = block * block_size
        places_here = start + jnp.arange(block_size)
        scores = jnp.einsum("hdt,hds->hts", queries, all_keys, preferred_element_type=jnp.float32)
        before = places_here[:, None] >= offsets[None, :]
        after = places_here[:, None] <= offsets[None, :]
        forward_decay_weight = jnp.exp(
            jnp.where(before, forward_prefix[:, :, None] - forward_prefix[:, None, :], -jnp.inf)
        )
        backward_weight = jnp.exp(
            jnp.where(after, backward_prefix[:, None, :] - backward_prefix[:, :, None], -jnp.inf)
        )
        weighted = (scores * (forward_decay_weight + backward_weight)).astype(jnp.bfloat16)
        inner = jnp.einsum("hts,hes->het", weighted, all_values, preferred_element_type=jnp.float32)
        query_wide = queries.astype(jnp.float32)
        carried = (
            jnp.einsum("hdt,hde->het", query_wide, forward_in) * jnp.exp(forward_prefix)[:, None, :]
        )
        carried = (
            carried
            + jnp.einsum("hdt,hde->het", query_wide, backward_in)
            * jnp.exp(backward_total[:, None] - backward_prefix)[:, None, :]
        )
        return inner + carried

    blocks = lax.map(block_output, jnp.arange(block_count))
    retained = jnp.transpose(blocks, (1, 2, 0, 3)).reshape(heads_here, HEAD_DIM, length)
    gate_values = gate_input.reshape(heads_here, HEAD_DIM, length).astype(jnp.float32)
    mixer_out = (
        (head_norm(retained, 1) * jax.nn.silu(gate_values))
        .reshape(heads_here * HEAD_DIM, length)
        .astype(jnp.bfloat16)
    )
    token_major = lax.all_to_all(mixer_out, TP, split_axis=1, concat_axis=0, tiled=True)
    projected = lax.dot_general(
        token_major, out_weight, (((0,), (0,)), ((), ())), preferred_element_type=jnp.float32
    )
    stream = residual.astype(jnp.float32) + projected
    scale = lax.rsqrt(jnp.mean(stream * stream, axis=-1, keepdims=True) + 1e-06)
    normed = (stream * scale * norm_gain.astype(jnp.float32)).astype(jnp.bfloat16)
    token_count = routes.shape[0]
    picks = routes.shape[1]
    width = normed.shape[1]
    experts_all = lax.axis_size("sp") * gate_weight.shape[0]
    capacity = (5 * token_count + 2 * experts_all - 1) // (2 * experts_all)
    flat_routes = routes.reshape(-1)
    matches = (flat_routes[:, None] == jnp.arange(experts_all)[None, :]).astype(jnp.int32)
    ranks = jnp.cumsum(matches, axis=0) - matches
    bucket_ordinal = jnp.sum(ranks * matches, axis=1)
    target = flat_routes * capacity + bucket_ordinal
    slot_grid = jnp.arange(experts_all * capacity)
    placing = (slot_grid[:, None] == target[None, :]).astype(jnp.int32)
    placing = jnp.sum(placing.reshape(experts_all * capacity, token_count, picks), axis=2).astype(
        jnp.bfloat16
    )
    send_rows = jnp.dot(placing, normed, preferred_element_type=jnp.float32).astype(jnp.bfloat16)
    send_rows = send_rows.reshape(experts_all, capacity, width)
    received = lax.all_to_all(send_rows, "sp", split_axis=0, concat_axis=0, tiled=True)
    piece = lax.all_gather(received, TP, axis=0, tiled=True)
    flat_rows = piece.reshape(-1, piece.shape[-1])
    gates = jnp.dot(flat_rows, gate_weight[0], preferred_element_type=jnp.float32)
    ups = jnp.dot(flat_rows, up_weight[0], preferred_element_type=jnp.float32)
    hidden = (jax.nn.silu(gates) * ups).astype(jnp.bfloat16)
    partial_out = jnp.dot(hidden, down_weight[0], preferred_element_type=jnp.float32).astype(
        jnp.bfloat16
    )
    partial_out = lax.optimization_barrier(partial_out)
    terms = partial_out.astype(jnp.float32).reshape(piece.shape)
    summed = sum_by_chip(terms.astype(jnp.bfloat16), "tp_0", "tp_1", 0).astype(jnp.float32)
    returned = lax.all_to_all(
        summed.astype(jnp.bfloat16), "sp", split_axis=0, concat_axis=0, tiled=True
    )
    flat_back = returned.reshape(experts_all * capacity, width)
    picked_rows = jnp.take(flat_back, target, axis=0).reshape(token_count, picks, width)
    combined = jnp.sum(route_weight[:, :, None] * picked_rows.astype(jnp.float32), axis=1)
    return (stream + combined).astype(jnp.bfloat16)


def solution(mesh):
    torus = Mesh(mesh.devices.reshape(mesh.shape["sp"], 8, 2), ("sp", "tp_0", "tp_1"))
    return jax.shard_map(
        on_device,
        mesh=torus,
        in_specs=(
            P(TP, "sp"),
            P(TP, "sp"),
            P(TP, "sp"),
            P(TP, "sp"),
            P(None, TP, "sp"),
            P(SP_TP, None),
            P(),
            P(),
            P(SP_TP, None),
            P(SP_TP, None),
            P("sp", None, TP),
            P("sp", None, TP),
            P("sp", TP, None),
        ),
        out_specs=P(SP_TP, None),
        check_vma=False,
    )
```

profile of v0, /device:TPU:1, one launch (start us, length us, event | category | flops | bytes accessed | tf_op | source)
XLA Modules:
  0.0 239.8 jit_solution(17017841697353408779)
XLA Ops:
  6.5 1.4 slice_reduce_fusion.2
  9.3 1.3 subtract_exponential_fusion
  13.9 0.9 convolution_convert_fusion.3
  14.9 0.9 convolution_convert_fusion.2
  16.2 20.0 %all_gather.6 = bf16[16,1,8194]{2,1,0:T(2,128)(2,1)S(1)} all-gather(bf16[1,1,8194]{2,1,0:T(2,128)(2,1)S(1)} %concatenate.3), channel_id=1, replica_groups=mesh['sp'=16,'tp_0'=8,'tp_1'=2] {'sp'}, dimensions={0}, use_global_device_ids=true | all-gather | bytes 278596 | tf_op jit(solution)/shard_map/all_gather | solution.py:15
  37.1 1.2 fusion.54
  40.3 1.8 fusion.29
  44.1 14.3 %all-to-all-start = ((bf16[16,2,512]{2,1,0:T(2,128)(2,1)}), bf16[16,2,512]{2,1,0:T(2,128)(2,1)S(1)}, u32[]{:S(2)}, u32[]{:S(2)}) async-start(bf16[16,2,512]{2,1,0:T(2,128)(2,1)} %reshape.562), calls=%async_computation | async-start | bytes 65536 | tf_op jit(solution)/shard_map/all_to_all | solution.py:145
  59.2 6.6 %all-to-all-done = bf16[16,2,512]{2,1,0:T(2,128)(2,1)S(1)} async-done(((bf16[16,2,512]{2,1,0:T(2,128)(2,1)}), bf16[16,2,512]{2,1,0:T(2,128)(2,1)S(1)}, u32[]{:S(2)}, u32[]{:S(2)}) %all-to-all-start) | async-done | bytes 32800 | tf_op jit(solution)/shard_map/all_to_all | solution.py:145
  66.1 3.0 %multiply_reduce_fusion.1 = (f32[16]{0:T(128)S(1)}, f32[16,2048]{1,0:T(8,128)S(1)}) fusion(bf16[1024,16]{0,1:T(8,128)(2,1)S(1)} %all_to_all.20, bf16[1024,2048]{1,0:T(8,128)(2,1)} %param.19, bf16[16,2048]{1,0:T(8,128)(2,1)S(1)} %copy-done.4), kind=kOutput, calls=%fused_computation.41 | convolution fusion | flops 67239920 | bytes 4423744 | tf_op jit(solution)/shard_map/dot_general | solution.py:146
  69.4 12.5 %all_to_all.26 = bf16[16,3,2048]{2,1,0:T(4,128)(2,1)S(1)} all-to-all(bf16[16,3,2048]{2,1,0:T(4,128)(2,1)S(1)} %reshape.542), channel_id=1, replica_groups=mesh['sp'=16,'tp_0'=8,'tp_1'=2] {'sp'}, dimensions={0} | all-to-all | bytes 393216 | tf_op jit(solution)/shard_map/all_to_all | solution.py:169
  82.0 0.8 copy.80
  83.0 34.4 %all-gather.2.cloned.1.call-done = bf16[256,3,2048]{2,0,1:T(8,128)(2,1)} async-done(((bf16[16,3,2048]{2,0,1:T(8,128)(2,1)}), bf16[256,3,2048]{2,0,1:T(8,128)(2,1)}) %all-gather.2.cloned.1.call-update) | async-done | bytes 3145744 | tf_op jit(solution)/shard_map/all_gather | solution.py:170
  117.4 6.5 %copy.81 = bf16[256,3,2048]{2,1,0:T(4,128)(2,1)} copy(bf16[256,3,2048]{2,0,1:T(8,128)(2,1)} %all-gather.2.cloned.1.call-done) | data formatting | bytes 6291456 | tf_op jit(solution)/shard_map/all_gather | solution.py:170
  123.9 8.8 %reshape.543 = bf16[768,2048]{1,0:T(8,128)(2,1)} reshape(bf16[256,3,2048]{2,1,0:T(4,128)(2,1)} %copy.81) | data formatting | bytes 6291456 | tf_op jit(solution)/shard_map/reshape | solution.py:171
  132.7 3.6 %fusion.3 = f32[768,344]{0,1:T(8,128)S(1)} fusion(bf16[768,2048]{1,0:T(8,128)(2,1)} %reshape.543, bf16[1,2048,344]{1,2,0:T(8,128)(2,1)} %param.23), kind=kOutput, calls=%fused_computation.7 | convolution fusion | flops 1082130432 | bytes 5611520 | tf_op jit(solution)/shard_map/dot_general | solution.py:172
  136.3 7.8 %convolution_convert_fusion = bf16[768,2048]{1,0:T(8,128)(2,1)} fusion(bf16[1,344,2048]{2,1,0:T(8,128)(2,1)S(1)} %copy-done, bf16[768,2048]{1,0:T(8,128)(2,1)} %reshape.543, bf16[1,2048,344]{1,2,0:T(8,128)(2,1)} %param.24, f32[768,344]{0,1:T(8,128)S(1)} %fusion.3), kind=kOutput, calls=%fused_computation.1 | convolution fusion | flops 2167418880 | bytes 10166272 | tf_op jit(solution)/shard_map/dot_general | solution.py:175
  144.1 9.1 %convert_element_type.160 = bf16[8,2,16,3,2048]{4,3,2,1,0:T(4,128)(2,1)} reshape(bf16[768,2048]{1,0:T(8,128)(2,1)} %convolution_convert_fusion) | data formatting | bytes 6291456 | tf_op jit(solution)/shard_map/convert_element_type | solution.py:180
  153.2 6.4 %copy.82 = bf16[2,8,16,3,2048]{4,2,3,1,0:T(8,128)(2,1)} copy(bf16[2,8,16,3,2048]{4,3,2,0,1:T(4,128)(2,1)} %bitcast.83) | data formatting | bytes 6291456 | tf_op jit(solution)/shard_map/transpose | solution.py:32
  159.7 15.0 %reduce-scatter.3.cloned.1.call-done = bf16[8,16,3,2048]{3,1,2,0:T(8,128)(2,1)} async-done(((bf16[16,16,3,2048]{3,1,2,0:T(8,128)(2,1)}), bf16[8,16,3,2048]{3,1,2,0:T(8,128)(2,1)}) %reduce-scatter.3.cloned.1.call-update) | async-done | bytes 1572880 | tf_op jit(solution)/shard_map/reduce_scatter | solution.py:33
  174.9 40.3 %reduce-scatter.5.cloned.1.call-done = bf16[1,16,3,2048]{3,1,2,0:T(8,128)(2,1)} async-done(((bf16[8,16,3,2048]{3,1,2,0:T(8,128)(2,1)}), bf16[1,16,3,2048]{3,1,2,0:T(8,128)(2,1)}) %reduce-scatter.5.cloned.1.call-update) | async-done | bytes 196624 | tf_op jit(solution)/shard_map/reduce_scatter | solution.py:34
  215.2 1.8 copy.83
  217.0 6.5 %all-to-all-start.2 = ((bf16[16,3,2048]{2,1,0:T(4,128)(2,1)}), bf16[16,3,2048]{2,1,0:T(4,128)(2,1)S(1)}, u32[]{:S(2)}, u32[]{:S(2)}) async-start(bf16[16,3,2048]{2,1,0:T(4,128)(2,1)} %copy.83), calls=%async_computation.4 | async-start | bytes 524288 | tf_op jit(solution)/shard_map/all_to_all | solution.py:181
  223.7 7.3 %all-to-all-done.2 = bf16[16,3,2048]{2,1,0:T(4,128)(2,1)S(1)} async-done(((bf16[16,3,2048]{2,1,0:T(4,128)(2,1)}), bf16[16,3,2048]{2,1,0:T(4,128)(2,1)S(1)}, u32[]{:S(2)}, u32[]{:S(2)}) %all-to-all-start.2) | async-done | bytes 196640 | tf_op jit(solution)/shard_map/all_to_all | solution.py:181
  (92 shorter events, 12.3 us)
Async XLA Ops:
  6.5 129.8 %copy-start = (bf16[1,344,2048]{2,1,0:T(8,128)(2,1)S(1)}, bf16[1,344,2048]{2,1,0:T(8,128)(2,1)}, u32[]{:S(2)}) copy-start(bf16[1,344,2048]{2,1,0:T(8,128)(2,1)} %param.25) | copy-start | bytes 4227076
  6.5 36.0 %copy-start.3 = (bf16[64,256]{1,0:T(8,128)(2,1)S(1)}, bf16[64,256]{1,0:T(8,128)(2,1)}, u32[]{:S(2)}) copy-start(bf16[64,256]{1,0:T(8,128)(2,1)} %param.14) | copy-start | bytes 98308
  6.5 36.0 %copy-start.2 = (bf16[64,256]{1,0:T(8,128)(2,1)S(1)}, bf16[64,256]{1,0:T(8,128)(2,1)}, u32[]{:S(2)}) copy-start(bf16[64,256]{1,0:T(8,128)(2,1)} %param.15) | copy-start | bytes 98308
  6.5 35.8 %copy-start.1 = (bf16[64,256]{1,0:T(8,128)(2,1)S(1)}, bf16[64,256]{1,0:T(8,128)(2,1)}, u32[]{:S(2)}) copy-start(bf16[64,256]{1,0:T(8,128)(2,1)} %param.13) | copy-start | bytes 98308
  14.9 28.2 %copy-start.5 = (bf16[64,256]{1,0:T(8,128)(2,1)S(1)}, bf16[64,256]{1,0:T(8,128)(2,1)}, u32[]{:S(2)}) copy-start(bf16[64,256]{1,0:T(8,128)(2,1)} %param.16) | copy-start | bytes 98308
  16.1 42.3 %copy-start.6 = (s32[16,2]{0,1:T(2,128)S(1)}, s32[16,2]{0,1:T(2,128)}, u32[]{:S(2)}) copy-start(s32[16,2]{0,1:T(2,128)} %param.21) | copy-start | bytes 388
  36.1 23.0 %copy-start.7 = (bf16[2048]{0:T(1024)(128)(2,1)S(1)}, bf16[2048]{0:T(1024)(128)(2,1)}, u32[]{:S(2)}) copy-start(bf16[2048]{0:T(1024)(128)(2,1)} %param.20) | copy-start | bytes 12292
  40.3 25.7 %copy-start.4 = (bf16[16,2048]{1,0:T(8,128)(2,1)S(1)}, bf16[16,2048]{1,0:T(8,128)(2,1)}, u32[]{:S(2)}) copy-start(bf16[16,2048]{1,0:T(8,128)(2,1)} %param.18) | copy-start | bytes 196612
  44.1 21.7 %all-to-all-start = ((bf16[16,2,512]{2,1,0:T(2,128)(2,1)}), bf16[16,2,512]{2,1,0:T(2,128)(2,1)S(1)}, u32[]{:S(2)}, u32[]{:S(2)}) async-start(bf16[16,2,512]{2,1,0:T(2,128)(2,1)} %reshape.562), calls=%async_computation | async-start | bytes 65536 | tf_op jit(solution)/shard_map/all_to_all | solution.py:145
  58.4 59.0 %all-gather.2.cloned.1.call-start = ((), (), s32[]{:S(2)}) async-start(), calls=%async_computation.5 | async-start | bytes 3342336 | tf_op jit(solution)/shard_map/all_gather | solution.py:170
  82.8 91.9 %reduce-scatter.3.cloned.1.call-start = ((), (), s32[]{:S(2)}) async-start(), calls=%async_computation.6 | async-start | bytes 4718592 | tf_op jit(solution)/shard_map/reduce_scatter | solution.py:33
  159.6 64.0 %copy-start.8 = (f32[16,2]{0,1:T(2,128)S(1)}, f32[16,2]{0,1:T(2,128)}, u32[]{:S(2)}) copy-start(f32[16,2]{0,1:T(2,128)} %param.22) | copy-start | bytes 388
  159.6 55.6 %reduce-scatter.5.cloned.1.call-start = ((), (), s32[]{:S(2)}) async-start(), calls=%async_computation.7 | async-start | bytes 1769472 | tf_op jit(solution)/shard_map/reduce_scatter | solution.py:34
  217.0 14.1 %all-to-all-start.2 = ((bf16[16,3,2048]{2,1,0:T(4,128)(2,1)}), bf16[16,3,2048]{2,1,0:T(4,128)(2,1)S(1)}, u32[]{:S(2)}, u32[]{:S(2)}) async-start(bf16[16,3,2048]{2,1,0:T(4,128)(2,1)} %copy.83), calls=%async_computation.4 | async-start | bytes 524288 | tf_op jit(solution)/shard_map/all_to_all | solution.py:181
Sparse Core Ops, SparseCore 0:
  82.9 34.4 all-gather.1
  159.7 14.9 reduce-scatter.2
  177.3 37.9 reduce-scatter.4
where the time goes:
time: 244 us; the launch traced here: 240 us
  waiting for transfers between devices  104 us (43%)
  local copies, waits for them, and re-layouts  39.6 us (16%)
  blocking collectives  32.5 us (13%)
  starting transfers between devices  21.1 us (9%)
  matrix products  17.1 us (7%)
  between operations  15.3 us (6%)
  other arithmetic  10.5 us (4%)
    reduce_scatter x1, waiting for transfers between devices, sum_by_chip(): return lax.psum_scatter(tiles, chips, scatter_dimension=0, tiled=True)[0]  40.3 us
    all_gather x1, waiting for transfers between devices, on_device(): piece = lax.all_gather(received, TP, axis=0, tiled=True)  34.4 us
    all_gather x1, blocking collectives, sent_together(): whole, at, done = (lax.all_gather(both, axis, axis=dim, tiled=True), 0, [])  20 us
    reduce_scatter x1, waiting for transfers between devices, sum_by_chip(): tiles = lax.psum_scatter(tiles, core, scatter_dimension=0, tiled=True)  15 us
    all_to_all x1, starting transfers between devices, on_device(): lax.all_to_all(mixer_out, TP, split_axis=1, concat_axis=0, tiled=True)  14.3 us
    all_to_all x1, blocking collectives, on_device(): lax.all_to_all(send_rows, 'sp', split_axis=0, concat_axis=0, tiled=True)  12.5 us
    convert_element_type x1, local copies, waits for them, and re-layouts, on_device(): terms.astype(jnp.bfloat16)  9.1 us
    reshape x1, local copies, waits for them, and re-layouts, on_device(): flat_rows = piece.reshape(-1, piece.shape[-1])  8.81 us
  transfers between devices with their start and end apart: 5, of which 5 were waited for; matrix products, arithmetic and copies ran while one was open for 0% of the time, Pallas kernels for 0%

commit v1 on v0

v1 whole, which is shorter than its diff:
```python
import functools

import jax
import jax.numpy as jnp
from jax import lax
from jax.experimental import pallas as pl
from jax.experimental.pallas import tpu as pltpu
from jax.sharding import PartitionSpec as P

HD = 64
D = 2048
FFD = 344
SP = 16
TPN = 16
NZ = 8
SEG = 256
TOK = 16
CAP = 3
ROWS = SP * CAP
HALF = D // 2
LANES = 128
NCH = D // LANES
F32 = jnp.float32
BF16 = jnp.bfloat16
MESH = pl.DeviceIdType.MESH


def contract(a, b, da, db):
    return lax.dot_general(a, b, (((da,), (db,)), ((), ())), preferred_element_type=F32)


def iota(shape, dim):
    return lax.broadcasted_iota(jnp.int32, shape, dim)


def kernel(
    q_ref,
    k_ref,
    v_ref,
    g_ref,
    ld_ref,
    res_ref,
    gain_ref,
    routes_ref,
    rw_ref,
    w_any,
    wg_any,
    wu_any,
    wd_any,
    out_ref,
    w_ref,
    wg_ref,
    wu_ref,
    wd_ref,
    st_ref,
    ysend_ref,
    yrecv_ref,
    stream_ref,
    tmp_ref,
    rsend_ref,
    rrecv_ref,
    ag_ref,
    part_ref,
    sib_ref,
    rs_send_ref,
    rs_recv_ref,
    bsend_ref,
    brecv_ref,
    wsem,
    st_ssem,
    st_rsem,
    y_ssem,
    y_rsem,
    r_ssem,
    r_rsem,
    ag_ssem,
    ag_rsem,
    mir_ssem,
    mir_rsem,
    sib_ssem,
    sib_rsem,
    rs_ssem,
    rs_rsem,
    b_ssem,
    b_rsem,
):
    me_s = lax.axis_index("sp")
    me_t = lax.axis_index("tp")
    z = me_t // 2
    core = me_t % 2
    other = 1 - core
    z_up = ((z + 1) % NZ) * 2 + core
    z_dn = ((z + NZ - 1) % NZ) * 2 + core
    sibling = z * 2 + other

    def remote(src, dst, ssem, rsem, where):
        return pltpu.make_async_remote_copy(
            src_ref=src, dst_ref=dst, send_sem=ssem, recv_sem=rsem, device_id=where, device_id_type=MESH
        )

    barrier = pltpu.get_barrier_semaphore()

    @pl.loop(1, SP)
    def _(j):
        pl.semaphore_signal(barrier, inc=1, device_id={"sp": (me_s + j) % SP}, device_id_type=MESH)
        pl.semaphore_signal(barrier, inc=1, device_id={"tp": (me_t + j) % TPN}, device_id_type=MESH)

    weights = [
        pltpu.make_async_copy(w_any, w_ref, wsem.at[0]),
        pltpu.make_async_copy(wg_any.at[0], wg_ref, wsem.at[1]),
        pltpu.make_async_copy(wu_any.at[0], wu_ref, wsem.at[2]),
        pltpu.make_async_copy(wd_any.at[0], wd_ref, wsem.at[3]),
    ]
    for copy in weights:
        copy.start()

    lf = ld_ref[0]
    lb = ld_ref[1]
    at_t = iota((SEG, SEG), 0)
    at_s = iota((SEG, SEG), 1)
    cf_col = jnp.sum(jnp.where(at_s <= at_t, lf, 0.0), axis=1, keepdims=True)
    eb_col = jnp.sum(jnp.where(at_s < at_t, lb, 0.0), axis=1, keepdims=True)
    cf = jnp.sum(jnp.where(at_s == at_t, cf_col, 0.0), axis=0, keepdims=True)
    eb = jnp.sum(jnp.where(at_s == at_t, eb_col, 0.0), axis=0, keepdims=True)
    total_f = jnp.sum(lf, axis=1, keepdims=True)
    total_b = jnp.sum(lb, axis=1, keepdims=True)
    q = q_ref[...]
    keys = k_ref[...]
    vals = v_ref[...]
    wide_keys = keys.astype(F32)
    kf = (wide_keys * jnp.exp(jnp.minimum(total_f - cf, 0.0))).astype(BF16)
    kb = (wide_keys * jnp.exp(eb)).astype(BF16)
    f_loc = contract(kf, vals, 1, 1)
    g_loc = contract(kb, vals, 1, 1)
    lane = iota((1, LANES), 1)
    totals = jnp.where(lane < HD, total_f, total_b)
    hi = totals.astype(BF16).astype(F32)
    mid = (totals - hi).astype(BF16).astype(F32)
    low = totals - hi - mid
    row16 = iota((16, LANES), 0)
    packed = jnp.where(row16 == 0, hi, jnp.where(row16 == 1, mid, jnp.where(row16 == 2, low, 0.0)))
    st_ref[me_s, pl.ds(0, HD), :] = jnp.concatenate([f_loc, g_loc], axis=1).astype(BF16)
    st_ref[me_s, pl.ds(HD, 16), :] = packed.astype(BF16)

    pl.semaphore_wait(barrier, 2 * (SP - 1))

    def st_copy(j):
        p = (me_s + j) % SP
        return remote(st_ref.at[me_s], st_ref.at[me_s], st_ssem.at[p], st_rsem.at[me_s], {"sp": p})

    @pl.loop(1, SP)
    def _(j):
        st_copy(j).start()

    scores = contract(q, keys, 0, 0)
    w = jnp.where(at_s <= at_t, jnp.exp(jnp.minimum(cf_col - cf, 0.0)), 0.0)
    w = w + jnp.where(at_s >= at_t, jnp.exp(jnp.minimum(eb - eb_col, 0.0)), 0.0)
    p_mat = (scores * w).astype(BF16)
    inner = contract(vals, p_mat, 1, 1)
    gates = g_ref[...].astype(F32)
    gate_act = gates * jax.nn.sigmoid(gates)

    def st_arrived(j):
        p = (me_s + j) % SP
        return remote(st_ref.at[p], st_ref.at[p], st_ssem.at[p], st_rsem.at[p], {"sp": p})

    @pl.loop(1, SP)
    def _(j):
        st_arrived(j).wait_recv()

    half_lane = iota((HD, LANES), 1) < HD

    def scan(i, acc):
        m_b = SP - 1 - i
        loc = jnp.where(half_lane, st_ref[i, pl.ds(0, HD), :].astype(F32), st_ref[m_b, pl.ds(0, HD), :].astype(F32))
        tail_f = jnp.sum(st_ref[i, pl.ds(HD, 16), :].astype(F32), axis=0, keepdims=True)
        tail_b = jnp.sum(st_ref[m_b, pl.ds(HD, 16), :].astype(F32), axis=0, keepdims=True)
        decay = jnp.exp(jnp.where(lane < HD, tail_f, tail_b))
        step_f = (i < me_s).astype(jnp.int32)
        step_b = (m_b > me_s).astype(jnp.int32)
        use = jnp.where(half_lane, step_f, step_b) > 0
        return jnp.where(use, decay * acc + loc, acc)

    state = lax.fori_loop(0, SP, scan, jnp.zeros((HD, LANES), F32))
    state_hi = state.astype(BF16)
    state_lo = (state - state_hi.astype(F32)).astype(BF16)
    carried = contract(state_hi, q, 0, 0) + contract(state_lo, q, 0, 0)
    o = inner + carried[:HD] * jnp.exp(cf) + carried[HD:] * jnp.exp(jnp.minimum(total_b - eb, 0.0))
    o = o - jnp.mean(o, axis=0, keepdims=True)
    o = o * lax.rsqrt(jnp.mean(o * o, axis=0, keepdims=True) + 1e-06)
    y = o * gate_act
    odd = core.astype(F32)
    both = jnp.concatenate([y * (1.0 - odd), y * odd], axis=0)
    ysend_ref[...] = jnp.transpose(both).astype(BF16).reshape(TPN, TOK, LANES)
    yrecv_ref[me_t] = ysend_ref[me_t]

    def y_copy(j):
        p = (me_t + j) % TPN
        return remote(ysend_ref.at[p], yrecv_ref.at[me_t], y_ssem.at[p], y_rsem.at[me_t], {"tp": p})

    @pl.loop(1, TPN)
    def _(j):
        y_copy(j).start()

    row_e = iota((ROWS, TOK), 0) // CAP
    row_r = iota((ROWS, TOK), 0) % CAP
    first = routes_ref[pl.ds(0, 1), :] == row_e
    named = jnp.logical_or(first, routes_ref[pl.ds(1, 1), :] == row_e)
    earlier = (iota((TOK, TOK), 0) < iota((TOK, TOK), 1)).astype(F32).astype(BF16)
    rank = jnp.dot(named.astype(F32).astype(BF16), earlier, preferred_element_type=F32)
    placed = jnp.logical_and(named, rank == row_r.astype(F32))
    placing = placed.astype(F32).astype(BF16)
    share = jnp.where(placed, jnp.where(first, rw_ref[pl.ds(0, 1), :], rw_ref[pl.ds(1, 1), :]), 0.0)
    share_hi = share.astype(BF16)
    share_lo = (share - share_hi.astype(F32)).astype(BF16)

    weights[0].wait()

    def y_arrived(j):
        p = (me_t + j) % TPN
        return remote(ysend_ref.at[p], yrecv_ref.at[p], y_ssem.at[p], y_rsem.at[p], {"tp": p})

    @pl.loop(1, TPN)
    def _(j):
        y_arrived(j).wait_recv()

    y_tok = jnp.concatenate([yrecv_ref[2 * i] + yrecv_ref[2 * i + 1] for i in range(NZ)], axis=1)
    square = jnp.zeros((TOK, 1), F32)
    for n in range(4):
        cols = pl.ds(n * 512, 512)
        part = res_ref[:, cols].astype(F32) + jnp.dot(y_tok, w_ref[:, cols], preferred_element_type=F32)
        stream_ref[:, cols] = part
        square = square + jnp.sum(part * part, axis=1, keepdims=True)
    scale = lax.rsqrt(square * (1.0 / D) + 1e-06)
    gain = gain_ref[...].astype(F32)
    for c in range(NCH):
        cols = pl.ds(c * LANES, LANES)
        normed = (stream_ref[:, cols] * scale * gain[c : c + 1, :]).astype(BF16)
        tmp_ref[:, c, :] = jnp.dot(placing, normed, preferred_element_type=F32)
    rsend_ref[...] = tmp_ref[...].astype(BF16)
    rrecv_ref[pl.ds(me_s * CAP, CAP)] = rsend_ref[pl.ds(me_s * CAP, CAP)]

    def r_copy(j):
        p = (me_s + j) % SP
        return remote(
            rsend_ref.at[pl.ds(p * CAP, CAP)], rrecv_ref.at[pl.ds(me_s * CAP, CAP)], r_ssem.at[p], r_rsem.at[me_s], {"sp": p}
        )

    @pl.loop(1, SP)
    def _(j):
        r_copy(j).start()

    def r_arrived(j):
        p = (me_s + j) % SP
        return remote(
            rsend_ref.at[pl.ds(p * CAP, CAP)], rrecv_ref.at[pl.ds(p * CAP, CAP)], r_ssem.at[p], r_rsem.at[p], {"sp": p}
        )

    @pl.loop(1, SP)
    def _(j):
        r_arrived(j).wait_recv()

    tmp_ref[...] = rrecv_ref[...].astype(F32)
    for c in range(NCH):
        ag_ref[0, core, :, pl.ds(c * LANES, LANES)] = tmp_ref[:, c, :].astype(BF16)

    def slot(d, k):
        return 0 if k == 0 else (7 if k == 4 else 2 * k - 1 + d)

    def hops(d, h):
        return 4 if d == h else 3

    def ag_send(d, h, k):
        cols = pl.ds(h * HALF, HALF)
        return remote(
            ag_ref.at[slot(d, k), core, :, cols],
            ag_ref.at[slot(d, k + 1), core, :, cols],
            ag_ssem.at[d, h, k],
            ag_rsem.at[d, h, k],
            {"tp": z_up if d == 0 else z_dn},
        )

    def mirror(d, h, k):
        cols = pl.ds(h * HALF, HALF)
        view = ag_ref.at[slot(d, k), core, :, cols]
        return remote(view, view, mir_ssem.at[d, h, k], mir_rsem.at[d, h, k], {"tp": sibling})

    def mirrored(d, h, k):
        cols = pl.ds(h * HALF, HALF)
        view = ag_ref.at[slot(d, k), other, :, cols]
        return remote(view, view, mir_ssem.at[d, h, k], mir_rsem.at[d, h, k], {"tp": sibling})

    def experts(s0, n):
        x = ag_ref[pl.ds(s0, n)].reshape(n * 2 * ROWS, D)
        a = contract(x, wg_ref[...], 1, 1)
        b = contract(x, wu_ref[...], 1, 1)
        hidden = (a * jax.nn.sigmoid(a) * b).astype(BF16)
        part_ref[pl.ds(s0, n)] = (
            jnp.dot(hidden, wd_ref[...], preferred_element_type=F32).astype(BF16).reshape(n, 2, ROWS, D)
        )

    def pair(s):
        return remote(part_ref.at[s, other], sib_ref.at[s], sib_ssem.at[s], sib_rsem.at[s], {"tp": sibling})

    for h in (0, 1):
        for d in (0, 1):
            ag_send(d, h, 0).start()
    for h in (0, 1):
        mirror(0, h, 0).start()
    for copy in weights[1:]:
        copy.wait()
    for h in (0, 1):
        mirrored(0, h, 0).wait_recv()
    experts(0, 1)
    pair(0).start()
    for k in range(1, 5):
        units = [(d, h) for (d, h) in ((0, 0), (1, 1), (0, 1), (1, 0)) if hops(d, h) >= k]
        for d, h in units:
            ag_send(d, h, k - 1).wait_recv()
            if hops(d, h) > k:
                ag_send(d, h, k).start()
            mirror(d, h, k).start()
        for d, h in units:
            mirrored(d, h, k).wait_recv()
        if k < 4:
            experts(2 * k - 1, 2)
            pair(2 * k - 1).start()
            pair(2 * k).start()
        else:
            experts(7, 1)
            pair(7).start()

    def rs_send(d, h, k):
        return remote(
            rs_send_ref.at[d, h, k - 1],
            rs_recv_ref.at[d, h, k - 1],
            rs_ssem.at[d, h, k - 1],
            rs_rsem.at[d, h, k - 1],
            {"tp": z_dn if d == 0 else z_up},
        )

    def pair_sum(s, h):
        cols = pl.ds(h * HALF, HALF)
        return part_ref[s, core, :, cols].astype(F32) + sib_ref[s, :, cols].astype(F32)

    def pair_arrived(s):
        pair(s).wait_recv()

    for s in range(8):
        pair_arrived(s)
    for k in range(4, 0, -1):
        fresh = [(d, h) for d in (0, 1) for h in (0, 1) if hops(d, h) == k]
        later = [(d, h) for d in (0, 1) for h in (0, 1) if hops(d, h) > k]
        if k < 3:
            later = [(0, 1), (1, 0), (0, 0), (1, 1)]
        for d, h in fresh + later:
            acc = pair_sum(slot(d, k), h)
            if (d, h) in later:
                rs_send(d, h, k + 1).wait_recv()
                acc = acc + rs_recv_ref[d, h, k].astype(F32)
            rs_send_ref[d, h, k - 1] = acc.astype(BF16)
            rs_send(d, h, k).start()
    for h in (0, 1):
        acc = pair_sum(0, h)
        for d in (0, 1):
            rs_send(d, h, 1).wait_recv()
            acc = acc + rs_recv_ref[d, h, 0].astype(F32)
        for c in range(NCH // 2):
            tmp_ref[:, h * (NCH // 2) + c, :] = acc[:, c * LANES : (c + 1) * LANES]
    bsend_ref[...] = tmp_ref[...].astype(BF16)
    brecv_ref[pl.ds(me_s * CAP, CAP)] = bsend_ref[pl.ds(me_s * CAP, CAP)]

    def b_copy(j):
        p = (me_s + j) % SP
        return remote(
            bsend_ref.at[pl.ds(p * CAP, CAP)], brecv_ref.at[pl.ds(me_s * CAP, CAP)], b_ssem.at[p], b_rsem.at[me_s], {"sp": p}
        )

    def b_arrived(j):
        p = (me_s + j) % SP
        return remote(
            bsend_ref.at[pl.ds(p * CAP, CAP)], brecv_ref.at[pl.ds(p * CAP, CAP)], b_ssem.at[p], b_rsem.at[p], {"sp": p}
        )

    @pl.loop(1, SP)
    def _(j):
        b_copy(j).start()

    @pl.loop(1, SP)
    def _(j):
        st_copy(j).wait_send()
        y_copy(j).wait_send()
        r_copy(j).wait_send()

    for d in (0, 1):
        for h in (0, 1):
            for k in range(hops(d, h)):
                ag_send(d, h, k).wait_send()
                rs_send(d, h, k + 1).wait_send()
                mirror(d, h, k + 1).wait_send()
    for h in (0, 1):
        mirror(0, h, 0).wait_send()
    for s in range(8):
        pair(s).wait_send()

    @pl.loop(1, SP)
    def _(j):
        b_arrived(j).wait_recv()

    tmp_ref[...] = brecv_ref[...].astype(F32)
    for c in range(NCH):
        cols = pl.ds(c * LANES, LANES)
        back = tmp_ref[:, c, :].astype(BF16)
        moe = contract(share_hi, back, 0, 0) + contract(share_lo, back, 0, 0)
        out_ref[:, cols] = (stream_ref[:, cols] + moe).astype(BF16)

    @pl.loop(1, SP)
    def _(j):
        b_copy(j).wait_send()


def on_device(q, k, v, g, ld, res, w, gain, routes, rw, wg, wu, wd):
    vmem = pl.BlockSpec(memory_space=pltpu.VMEM)
    hbm = pl.BlockSpec(memory_space=pl.ANY)
    dma = pltpu.SemaphoreType.DMA
    return pl.pallas_call(
        kernel,
        out_shape=jax.ShapeDtypeStruct((TOK, D), BF16),
        in_specs=[vmem] * 9 + [hbm] * 4,
        out_specs=vmem,
        scratch_shapes=[
            pltpu.VMEM((1024, D), BF16),
            pltpu.VMEM((FFD, D), BF16),
            pltpu.VMEM((FFD, D), BF16),
            pltpu.VMEM((FFD, D), BF16),
            pltpu.VMEM((SP, HD + 16, LANES), BF16),
            pltpu.VMEM((TPN, TOK, LANES), BF16),
            pltpu.VMEM((TPN, TOK, LANES), BF16),
            pltpu.VMEM((TOK, D), F32),
            pltpu.VMEM((ROWS, NCH, LANES), F32),
            pltpu.VMEM((ROWS, NCH, LANES), BF16),
            pltpu.VMEM((ROWS, NCH, LANES), BF16),
            pltpu.VMEM((8, 2, ROWS, D), BF16),
            pltpu.VMEM((8, 2, ROWS, D), BF16),
            pltpu.VMEM((8, ROWS, D), BF16),
            pltpu.VMEM((2, 2, 4, ROWS, HALF), BF16),
            pltpu.VMEM((2, 2, 4, ROWS, HALF), BF16),
            pltpu.VMEM((ROWS, NCH, LANES), BF16),
            pltpu.VMEM((ROWS, NCH, LANES), BF16),
            dma((4,)),
            dma((SP,)),
            dma((SP,)),
            dma((TPN,)),
            dma((TPN,)),
            dma((SP,)),
            dma((SP,)),
            dma((2, 2, 4)),
            dma((2, 2, 4)),
            dma((2, 2, 5)),
            dma((2, 2, 5)),
            dma((8,)),
            dma((8,)),
            dma((2, 2, 4)),
            dma((2, 2, 4)),
            dma((SP,)),
            dma((SP,)),
        ],
        compiler_params=pltpu.CompilerParams(
            collective_id=0, has_side_effects=True, vmem_limit_bytes=60 * 1024 * 1024
        ),
    )(
        q,
        k,
        v,
        g,
        ld,
        res,
        gain.reshape(NCH, LANES),
        routes.T,
        rw.T,
        w,
        jnp.swapaxes(wg, 1, 2),
        jnp.swapaxes(wu, 1, 2),
        wd,
    )


def solution(mesh):
    return jax.shard_map(
        on_device,
        mesh=mesh,
        in_specs=(
            P("tp", "sp"),
            P("tp", "sp"),
            P("tp", "sp"),
            P("tp", "sp"),
            P(None, "tp", "sp"),
            P(("sp", "tp"), None),
            P(),
            P(),
            P(("sp", "tp"), None),
            P(("sp", "tp"), None),
            P("sp", None, "tp"),
            P("sp", None, "tp"),
            P("sp", "tp", None),
        ),
        out_specs=P(("sp", "tp"), None),
        check_vma=False,
    )
```

time: 244 us -> 80.7 us (0.33); the launches traced: 240 us -> 80.5 us
  waiting for transfers between devices: 104 us -> 0 us
  Pallas kernels: 0 us -> 79 us
  local copies, waits for them, and re-layouts: 39.6 us -> 1.47 us
  blocking collectives: 32.5 us -> 0 us
  starting transfers between devices: 21.1 us -> 0 us
  matrix products: 17.1 us -> 0 us
  between operations: 15.3 us -> 0.01 us
  other arithmetic: 10.5 us -> 0 us
    pallas_call x0 -> x1, Pallas kernels: none -> 79 us  [on_device(): pl.pallas_call(kernel, out_shape=jax.ShapeDtypeStruct((TOK, D), BF16), in...]
    reduce_scatter x2 -> x0, waiting for transfers between devices: 55.3 us -> none  [the longest x1 40.3 us: sum_by_chip(): return lax.psum_scatter(tiles, chips, scatter_dimension=0, tiled=True)[0]]
    all_gather x1 -> x0, waiting for transfers between devices: 34.4 us -> none  [on_device(): piece = lax.all_gather(received, TP, axis=0, tiled=True)]
    all_to_all x2 -> x0, starting transfers between devices: 20.8 us -> none  [the longest x1 14.3 us: on_device(): lax.all_to_all(mixer_out, TP, split_axis=1, concat_axis=0, tiled=True)]
    all_gather x1 -> x0, blocking collectives: 20 us -> none  [sent_together(): whole, at, done = (lax.all_gather(both, axis, axis=dim, tiled=True), 0, [])]
    dot_general x9 -> x0, matrix products: 17.1 us -> none  [the longest x1 7.76 us: on_device(): jnp.dot(hidden, down_weight[0], preferred_element_type=jnp.float32)]
    all_to_all x2 -> x0, waiting for transfers between devices: 13.9 us -> none  [the longest x1 7.34 us: on_device(): lax.all_to_all(summed.astype(jnp.bfloat16), 'sp', split_axis=0, concat_ax...]
    all_to_all x1 -> x0, blocking collectives: 12.5 us -> none  [on_device(): lax.all_to_all(send_rows, 'sp', split_axis=0, concat_axis=0, tiled=True)]
  transfers between devices with their start and end apart: 5 -> 0, of which waited for: 5 -> 0; matrix products, arithmetic and copies ran while one was open for 0% -> 0% of each run, Pallas kernels for 0% -> 0%
where the time goes in v1:
time: 80.7 us; the launch traced here: 80.5 us
  Pallas kernels  79 us (98%)
  local copies, waits for them, and re-layouts  1.47 us (2%)
    pallas_call x1, Pallas kernels, on_device(): pl.pallas_call(kernel, out_shape=jax.ShapeDtypeStruct((TOK, D), BF16), in...  79 us

profile of v1, /device:TPU:1, one launch (start us, length us, event | category | flops | bytes accessed | tf_op | source)
XLA Modules:
  0.0 80.5 jit_solution(13724979486922177901)
XLA Ops:
  0.0 79.0 %shard_map.127 = bf16[16,2048]{1,0:T(8,128)(2,1)} custom-call(bf16[64,256]{1,0:T(8,128)(2,1)} %q_ref.1, bf16[64,256]{1,0:T(8,128)(2,1)} %k_ref.1, bf16[64,256]{1,0:T(8,128)(2,1)} %v_ref.1, bf16[64,256]{1,0:T(8,128)(2,1)} %g_ref.1, f32[2,1,256]{2,1,0:T(1,128)} %ld_ref.1, bf16[16,2048]{1,0:T(8,128)(2,1)} %res_ref.1, bf16[16,128]{1,0:T(8,128)(2,1)} %bitcast.7, ...), custom_call_target="tpu_custom_call" | custom-call | tf_op jit(solution)/shard_map/pallas_call | solution.py:426
  79.0 1.5 %copy.15 = bf16[16,2048]{1,0:T(8,128)(2,1)} copy(bf16[16,2048]{1,0:T(8,128)(2,1)} %shard_map.127) | data formatting | bytes 131072
